TPU v7x, 32 devices: a whole 2x2x4 slice. The times are simulated.
32 devices in a mesh: sp: 4 (over z), fs: 4 (over y, x), tp: 2 (over core).
Axes of the slice: x: 2, y: 2, z: 4, core: 2. Of those that a mesh axis runs over, the one named last changes fastest.
Arguments:
- tokens: bfloat16 [4, 1024, 2048], P('fs', ('sp', 'tp')), may hold values from -6 to 6
- query_weight: bfloat16 [2048, 2048], P(('sp', 'fs'), 'tp'), may hold values from -0.125 to 0.125
- forget_weight: bfloat16 [2048, 2048], P(('sp', 'fs'), 'tp'), may hold values from -0.125 to 0.125
- value_weight: bfloat16 [2048, 2048], P(('sp', 'fs'), 'tp'), may hold values from -0.125 to 0.125
- convolution_gate_weight: bfloat16 [2048, 1024], P(('sp', 'fs'), 'tp'), may hold values from -0.125 to 0.125
- convolution_multiplier_weight: bfloat16 [2048, 1024], P(('sp', 'fs'), 'tp'), may hold values from -0.125 to 0.125
- convolution_input_weight: bfloat16 [2048, 1024], P(('sp', 'fs'), 'tp'), may hold values from -0.125 to 0.125
- gate_headroom: float32 [2048], P('tp'), may hold values from 9.765625e-05 to 0.06
- added_log_rate: float32 [4, 16, 1024], P('fs', 'tp', 'sp'), may hold values from -1.6 to 0
- initial_state: float32 [4, 16, 128, 128], P('fs', 'tp'), may hold values from -0.5 to 0.5
- head_norm_gain: float32 [2048], P('tp'), may hold values from 0.1 to 1.9
- convolution_taps: float32 [3, 1024], P(None, 'tp'), may hold values from -3.5 to 3.5
- convolution_bias: float32 [1024], P('tp'), may hold values from -4 to 4
- recurrence_output_weight: bfloat16 [2048, 2048], P('tp', ('sp', 'fs')), may hold values from -0.109375 to 0.109375
- convolution_output_weight: bfloat16 [1024, 2048], P('tp', ('sp', 'fs')), may hold values from -0.109375 to 0.109375
Outputs:
- mixed: bfloat16 [4, 1024, 2048], P('fs', ('sp', 'tp'))
All inputs are finite; a program needn't handle non-finite values.
Results may differ from a plain program's by a relative error of at most 0.018.
Values may be sent and summed in bfloat16 or wider, within the bound.
A program may use at most 64 MiB of HBM per device.

v0:
```python
import jax
import jax.numpy as jnp
from jax import lax
from jax.sharding import PartitionSpec as P

DK = 128
KW = 3
BLOCK_POSITIONS = 64


def carried_in(part, axis, combine, identity):
    place = lax.axis_index(axis)
    gathered = jax.tree.map(lambda a: lax.all_gather(a, axis), part)
    state = jax.tree.map(lambda a, e: jnp.zeros_like(a) + jnp.asarray(e, a.dtype), part, identity)

    def one(hop, state):
        return combine(
            state, jax.tree.map(lambda a: lax.dynamic_index_in_dim(a, hop, 0, False), gathered)
        )

    return lax.fori_loop(0, place, one, state)


def from_behind(block, axis, distance):
    devices = range(lax.axis_size(axis))
    route = [(i - distance, i) for i in devices if i - distance in devices]
    return lax.ppermute(block, axis, route)


def to_blocks(values, number_of_heads):
    number_of_blocks = values.shape[0] // BLOCK_POSITIONS
    return jnp.transpose(
        values.reshape(number_of_blocks, BLOCK_POSITIONS, number_of_heads, DK), (2, 0, 1, 3)
    )


def within_block_recurrence(
    query_vectors, forget_logits, value_vectors, gate_headroom, extra_rates
):
    number_of_heads = extra_rates.shape[0]
    number_of_blocks = query_vectors.shape[0] // BLOCK_POSITIONS
    query_scaled = to_blocks(query_vectors.astype(jnp.float32), number_of_heads) * DK ** (-0.5)
    gated_key = to_blocks(
        gate_headroom[None, :] * jax.nn.sigmoid(-forget_logits.astype(jnp.float32)), number_of_heads
    )
    forget_log_rate = (
        jnp.log1p(-gated_key)
        + extra_rates.reshape(number_of_heads, number_of_blocks, BLOCK_POSITIONS)[..., None]
    )
    values = to_blocks(value_vectors.astype(jnp.float32), number_of_heads)
    cumulative = jnp.cumsum(forget_log_rate, axis=2)
    query_decayed = query_scaled * jnp.exp(cumulative)
    key_decayed = gated_key * jnp.exp(-cumulative)
    scores = jnp.einsum(
        "hnik,hnjk->hnij", query_decayed, key_decayed, precision=lax.Precision.HIGHEST
    )
    causal = jnp.tril(jnp.ones((BLOCK_POSITIONS, BLOCK_POSITIONS), dtype=bool))
    scores = jnp.where(causal, scores, 0.0)
    within = jnp.einsum("hnij,hnjv->hniv", scores, values, precision=lax.Precision.HIGHEST)
    final_log = cumulative[:, :, -1, :]
    contrib = jnp.einsum(
        "hnck,hncv->hnkv",
        gated_key * jnp.exp(final_log[:, :, None, :] - cumulative),
        values,
        precision=lax.Precision.HIGHEST,
    )
    decays = jnp.exp(final_log)

    def advance(current, block_pair):
        return (block_pair[0][..., None] * current + block_pair[1], current)

    empty_state = jnp.zeros((number_of_heads, DK, DK), jnp.float32)
    local_total, entering = lax.scan(
        advance, empty_state, (jnp.moveaxis(decays, 1, 0), jnp.moveaxis(contrib, 1, 0))
    )
    entering = jnp.moveaxis(entering, 0, 1)
    before = jnp.exp(jnp.cumsum(final_log, axis=1) - final_log)
    device_decay = jnp.exp(jnp.sum(final_log, axis=1))
    return (query_decayed, within, entering, before, device_decay, local_total)


def finish(query_decayed, within, entering, before, carried, head_norm_gain):
    number_of_heads = query_decayed.shape[0]
    states = entering + before[..., None] * carried[:, None]
    carried_term = jnp.einsum(
        "hnck,hnkv->hncv", query_decayed, states, precision=lax.Precision.HIGHEST
    )
    length = query_decayed.shape[1] * BLOCK_POSITIONS
    recurrence_unnormed = jnp.transpose(within + carried_term, (1, 2, 0, 3)).reshape(
        length, number_of_heads, DK
    )
    mean_square = jnp.mean(recurrence_unnormed * recurrence_unnormed, axis=-1, keepdims=True)
    rec_out = (
        recurrence_unnormed
        * lax.rsqrt(mean_square + 1e-06)
        * head_norm_gain.reshape(number_of_heads, DK)
    )
    return rec_out.reshape(length, number_of_heads * DK).astype(jnp.bfloat16)


def chain_combine(earlier_part, later_part):
    return (
        earlier_part[0] * later_part[0],
        later_part[0][..., None] * earlier_part[1] + later_part[1],
    )


def shards(
    tokens,
    query_weight,
    forget_weight,
    value_weight,
    convolution_gate_weight,
    convolution_multiplier_weight,
    convolution_input_weight,
    gate_headroom,
    added_log_rate,
    initial_state,
    head_norm_gain,
    convolution_taps,
    convolution_bias,
    recurrence_output_weight,
    convolution_output_weight,
):
    own_rows = tokens[0]
    gathered = (
        lax.all_gather(query_weight, ("sp", "fs"), axis=0, tiled=True),
        lax.all_gather(forget_weight, ("sp", "fs"), axis=0, tiled=True),
        lax.all_gather(value_weight, ("sp", "fs"), axis=0, tiled=True),
        lax.all_gather(convolution_gate_weight, ("sp", "fs"), axis=0, tiled=True),
        lax.all_gather(convolution_multiplier_weight, ("sp", "fs"), axis=0, tiled=True),
        lax.all_gather(convolution_input_weight, ("sp", "fs"), axis=0, tiled=True),
        lax.all_gather(recurrence_output_weight, ("sp", "fs"), axis=1, tiled=True),
        lax.all_gather(convolution_output_weight, ("sp", "fs"), axis=1, tiled=True),
    )
    in_weights = gathered[:6]
    out_rec = gathered[6]
    out_conv = gathered[7]
    block_rows = lax.all_gather(own_rows, "tp", axis=0, tiled=True)
    projected = jnp.concatenate(
        [
            jnp.dot(block_rows, weight, preferred_element_type=jnp.float32).astype(jnp.bfloat16)
            for weight in in_weights
        ],
        axis=1,
    )
    rec_width = query_weight.shape[1]
    conv_width = convolution_gate_weight.shape[1]
    query_vectors = projected[:, :rec_width]
    forget_logits = projected[:, rec_width : 2 * rec_width]
    value_vectors = projected[:, 2 * rec_width : 3 * rec_width]
    conv_base = 3 * rec_width
    conv_gate = projected[:, conv_base : conv_base + conv_width]
    conv_mult = projected[:, conv_base + conv_width : conv_base + 2 * conv_width]
    conv_input = projected[:, conv_base + 2 * conv_width : conv_base + 3 * conv_width]
    query_decayed, within, entering, before, device_decay, local_total = within_block_recurrence(
        query_vectors, forget_logits, value_vectors, gate_headroom, added_log_rate[0]
    )
    conv_prod = conv_mult.astype(jnp.float32) * conv_input.astype(jnp.float32)
    length = conv_prod.shape[0]
    tail_rows = conv_prod[length - (KW - 1) :]
    unit_decay = jnp.ones_like(device_decay)
    empty_state = jnp.zeros_like(local_total)
    prior_decay, prior_state = carried_in(
        (device_decay, local_total), "sp", chain_combine, (unit_decay, empty_state)
    )
    prior_rows = from_behind(tail_rows, "sp", 1)
    carried = prior_decay[..., None] * initial_state[0] + prior_state
    rec_out = finish(query_decayed, within, entering, before, carried, head_norm_gain)
    extended = jnp.concatenate([prior_rows, conv_prod], axis=0)
    conv_y = jnp.broadcast_to(convolution_bias[None, :], conv_prod.shape)
    for j in range(KW):
        conv_y = conv_y + convolution_taps[j][None, :] * extended[j : j + length]
    conv_out = (conv_gate.astype(jnp.float32) * conv_y).astype(jnp.bfloat16)
    mixed = lax.psum_scatter(
        (
            jnp.dot(rec_out, out_rec, preferred_element_type=jnp.float32)
            + jnp.dot(conv_out, out_conv, preferred_element_type=jnp.float32)
        ).astype(jnp.bfloat16),
        "tp",
        scatter_dimension=0,
        tiled=True,
    )
    return mixed[None]


def solution(mesh):
    in_specs = (
        P("fs", ("sp", "tp"), None),
        P(("sp", "fs"), "tp"),
        P(("sp", "fs"), "tp"),
        P(("sp", "fs"), "tp"),
        P(("sp", "fs"), "tp"),
        P(("sp", "fs"), "tp"),
        P(("sp", "fs"), "tp"),
        P("tp"),
        P("fs", "tp", "sp"),
        P("fs", "tp", None, None),
        P("tp"),
        P(None, "tp"),
        P("tp"),
        P("tp", ("sp", "fs")),
        P("tp", ("sp", "fs")),
    )
    out_specs = P("fs", ("sp", "tp"), None)
    return jax.shard_map(shards, mesh=mesh, in_specs=in_specs, out_specs=out_specs, check_vma=False)
```

profile of v0, /device:TPU:28, one launch (start us, length us, event | category | flops | bytes accessed | tf_op | source)
XLA Modules:
  0.0 656.9 jit_solution(4386405157501010555)
XLA Ops:
  11.5 7.7 %all-gather.30.cloned.1.call-done = bf16[1,256,2048]{2,1,0:T(8,128)(2,1)} async-done(((bf16[1,128,2048]{2,1,0:T(8,128)(2,1)}), bf16[1,256,2048]{2,1,0:T(8,128)(2,1)}) %all-gather.30.cloned.1.call-update) | async-done | bytes 1048592 | tf_op jit(solution)/shard_map/all_gather | solution.py:139
  19.1 77.9 %all-gather.14.cloned.1.call-done = bf16[2048,1024]{1,0:T(8,128)(2,1)} async-done(((bf16[128,1024]{1,0:T(8,128)(2,1)}), bf16[2048,1024]{1,0:T(8,128)(2,1)}) %all-gather.14.cloned.1.call-update) | async-done | bytes 4194320 | tf_op jit(solution)/shard_map/all_gather | solution.py:127
  97.0 3.8 fusion.17
  100.8 73.2 %all-gather.16.cloned.1.call-done = bf16[2048,1024]{1,0:T(8,128)(2,1)} async-done(((bf16[128,1024]{1,0:T(8,128)(2,1)}), bf16[2048,1024]{1,0:T(8,128)(2,1)}) %all-gather.16.cloned.1.call-update) | async-done | bytes 4194320 | tf_op jit(solution)/shard_map/all_gather | solution.py:128
  174.0 4.5 fusion.14
  178.6 72.3 %all-gather.18.cloned.1.call-done = bf16[2048,1024]{1,0:T(8,128)(2,1)} async-done(((bf16[128,1024]{1,0:T(8,128)(2,1)}), bf16[2048,1024]{1,0:T(8,128)(2,1)}) %all-gather.18.cloned.1.call-update) | async-done | bytes 4194320 | tf_op jit(solution)/shard_map/all_gather | solution.py:129
  250.9 3.5 fusion.18
  255.7 1.8 bitcast_multiply_fusion.1
  257.5 2.1 convolution_bitcast_fusion
  259.6 4.6 while.26
  260.8 0.9 bitcast_dynamic-update-slice_fusion.2
  267.2 45.5 %all-gather.26.cloned.1.call-done = bf16[2048,512]{1,0:T(8,128)(2,1)} async-done(((bf16[128,512]{1,0:T(8,128)(2,1)}), bf16[2048,512]{1,0:T(8,128)(2,1)}) %all-gather.26.cloned.1.call-update) | async-done | bytes 2097168 | tf_op jit(solution)/shard_map/all_gather | solution.py:132
  312.7 2.6 fusion.22
  315.3 59.2 %all-gather.24.cloned.1.call-done = bf16[2048,512]{1,0:T(8,128)(2,1)} async-done(((bf16[128,512]{1,0:T(8,128)(2,1)}), bf16[2048,512]{1,0:T(8,128)(2,1)}) %all-gather.24.cloned.1.call-update) | async-done | bytes 2097168 | tf_op jit(solution)/shard_map/all_gather | solution.py:131
  374.5 2.4 fusion.21
  377.0 1.3 collective-permute-start
  378.3 14.5 %all-gather.1 = f32[32,128]{1,0:T(8,128)S(1)} all-gather(f32[8,128]{1,0:T(8,128)S(1)} %exp.41), channel_id=3, replica_groups=mesh['sp'=4,'fs'=4,'tp'=2] {'sp'}, dimensions={0}, use_global_device_ids=true | all-gather | bytes 20480 | tf_op jit(solution)/shard_map/all_gather | solution.py:13
  392.8 0.8 fusion.23
  393.6 2.9 convolution_select_fusion
  397.2 22.6 %all-gather.32.cloned.1.call-done = f32[32,128,128]{2,1,0:T(8,128)} async-done(((f32[8,128,128]{2,1,0:T(8,128)}), f32[32,128,128]{2,1,0:T(8,128)}) %all-gather.32.cloned.1.call-update) | async-done | bytes 2097168 | tf_op jit(solution)/shard_map/all_gather | solution.py:13
  419.8 4.1 while.25
  419.9 1.4 bitcast_add_fusion.7
  421.3 1.3 bitcast_add_fusion.7
  422.7 1.3 bitcast_add_fusion.7
  424.2 5.1 multiply_reduce_fusion
  429.4 1.8 copy.43
  431.3 79.0 %all-gather.20.cloned.1.call-done = bf16[1024,2048]{1,0:T(8,128)(2,1)} async-done(((bf16[1024,128]{1,0:T(8,128)(2,1)}), bf16[1024,2048]{1,0:T(8,128)(2,1)}) %all-gather.20.cloned.1.call-update) | async-done | bytes 4194320 | tf_op jit(solution)/shard_map/all_gather | solution.py:133
  510.6 3.6 fusion.48
  514.2 58.1 %all-gather.22.cloned.1.call-done = bf16[2048,512]{1,0:T(8,128)(2,1)} async-done(((bf16[128,512]{1,0:T(8,128)(2,1)}), bf16[2048,512]{1,0:T(8,128)(2,1)}) %all-gather.22.cloned.1.call-update) | async-done | bytes 2097168 | tf_op jit(solution)/shard_map/all_gather | solution.py:130
  572.3 63.6 %all-gather.28.cloned.1.call-done = bf16[512,2048]{1,0:T(8,128)(2,1)} async-done(((bf16[512,128]{1,0:T(8,128)(2,1)}), bf16[512,2048]{1,0:T(8,128)(2,1)}) %all-gather.28.cloned.1.call-update) | async-done | bytes 2097168 | tf_op jit(solution)/shard_map/all_gather | solution.py:134
  636.0 5.5 fusion
  641.5 8.9 %reduce-scatter.2.cloned.1.call-done = bf16[128,2048]{1,0:T(8,128)(2,1)} async-done(((bf16[256,2048]{1,0:T(8,128)(2,1)}), bf16[128,2048]{1,0:T(8,128)(2,1)}) %reduce-scatter.2.cloned.1.call-update) | async-done | bytes 524304 | tf_op jit(solution)/shard_map/reduce_scatter | solution.py:175
  (84 shorter events, 14.0 us)
Async XLA Ops:
  6.5 12.6 %all-gather.30.cloned.1.call-start = ((), (), s32[]{:S(2)}) async-start(), calls=%async_computation.10 | async-start | bytes 1572864 | tf_op jit(solution)/shard_map/all_gather | solution.py:139
  7.3 89.8 %all-gather.14.cloned.1.call-start = ((), (), s32[]{:S(2)}) async-start(), calls=%async_computation.1 | async-start | bytes 4456448 | tf_op jit(solution)/shard_map/all_gather | solution.py:127
  8.0 166.0 %all-gather.16.cloned.1.call-start = ((), (), s32[]{:S(2)}) async-start(), calls=%async_computation.2 | async-start | bytes 4456448 | tf_op jit(solution)/shard_map/all_gather | solution.py:128
  8.7 242.1 %all-gather.18.cloned.1.call-start = ((), (), s32[]{:S(2)}) async-start(), calls=%async_computation.3 | async-start | bytes 4456448 | tf_op jit(solution)/shard_map/all_gather | solution.py:129
  9.3 303.4 %all-gather.26.cloned.1.call-start = ((), (), s32[]{:S(2)}) async-start(), calls=%async_computation.7 | async-start | bytes 2228224 | tf_op jit(solution)/shard_map/all_gather | solution.py:132
  9.9 364.6 %all-gather.24.cloned.1.call-start = ((), (), s32[]{:S(2)}) async-start(), calls=%async_computation.6 | async-start | bytes 2228224 | tf_op jit(solution)/shard_map/all_gather | solution.py:131
  10.5 409.3 %all-gather.32.cloned.1.call-start = ((), (), s32[]{:S(2)}) async-start(), calls=%async_computation.11 | async-start | bytes 2621440 | tf_op jit(solution)/shard_map/all_gather | solution.py:13
  11.4 162.6 %copy-start.12 = (f32[1024]{0:T(1024)S(1)}, f32[1024]{0:T(1024)}, u32[]{:S(2)}) copy-start(f32[1024]{0:T(1024)} %param.26) | copy-start | bytes 12292
  19.1 154.9 %copy-start.3 = (bf16[1,256,2048]{2,1,0:T(8,128)(2,1)S(1)}, bf16[1,256,2048]{2,1,0:T(8,128)(2,1)}, u32[]{:S(2)}) copy-start(bf16[1,256,2048]{2,1,0:T(8,128)(2,1)} %all-gather.30.cloned.1.call-done) | copy-start | bytes 3145732
  250.9 3.5 copy-start.7
  255.6 1.8 copy-start.2
  259.6 7.6 %copy-start.10 = (f32[3,512]{1,0:T(4,128)S(1)}, f32[3,512]{1,0:T(4,128)}, u32[]{:S(2)}) copy-start(f32[3,512]{1,0:T(4,128)} %param.30) | copy-start | bytes 18436
  264.2 0.8 copy-start
  265.0 109.5 %copy-start.4 = (bf16[1,256,2048]{2,1,0:T(8,128)(2,1)S(1)}, bf16[1,256,2048]{2,1,0:T(8,128)(2,1)}, u32[]{:S(2)}) copy-start(bf16[1,256,2048]{2,1,0:T(8,128)(2,1)} %all-gather.30.cloned.1.call-done) | copy-start | bytes 3145732
  265.0 245.2 %all-gather.20.cloned.1.call-start = ((), (), s32[]{:S(2)}) async-start(), calls=%async_computation.4 | async-start | bytes 4456448 | tf_op jit(solution)/shard_map/all_gather | solution.py:133
  265.8 306.5 %all-gather.22.cloned.1.call-start = ((), (), s32[]{:S(2)}) async-start(), calls=%async_computation.5 | async-start | bytes 2228224 | tf_op jit(solution)/shard_map/all_gather | solution.py:130
  266.5 369.4 %all-gather.28.cloned.1.call-start = ((), (), s32[]{:S(2)}) async-start(), calls=%async_computation.8 | async-start | bytes 2228224 | tf_op jit(solution)/shard_map/all_gather | solution.py:134
  267.1 383.3 %reduce-scatter.2.cloned.1.call-start = ((), (), s32[]{:S(2)}) async-start(), calls=%async_computation.9 | async-start | bytes 1572864 | tf_op jit(solution)/shard_map/reduce_scatter | solution.py:175
  315.3 78.3 %copy-start.1 = (f32[8,4,64,128]{3,0,1,2:T(8,128)S(1)}, f32[8,4,64,128]{3,0,1,2:T(8,128)}, u32[]{:S(2)}) copy-start(f32[8,4,64,128]{3,0,1,2:T(8,128)} %get-tuple-element.132) | copy-start | bytes 3145732
  374.5 19.1 %copy-start.5 = (f32[8,4,64,128]{3,0,1,2:T(8,128)S(1)}, f32[8,4,64,128]{3,0,1,2:T(8,128)}, u32[]{:S(2)}) copy-start(f32[8,4,64,128]{3,0,1,2:T(8,128)} %get-tuple-element.129) | copy-start | bytes 3145732
  376.9 16.7 %copy-start.6 = (f32[256,512]{1,0:T(8,128)}, f32[256,512]{1,0:T(8,128)S(1)}, u32[]{:S(2)}) copy-start(f32[256,512]{1,0:T(8,128)S(1)} %fusion.21) | copy-start | bytes 1572868
  377.0 259.0 %collective-permute-start = (f32[2,512]{1,0:T(2,128)S(1)}, f32[2,512]{1,0:T(2,128)S(1)}, u32[]{:S(2)}, u32[]{:S(2)}) collective-permute-start(f32[2,512]{1,0:T(2,128)S(1)} %slice.29), channel_id=1, source_target_pairs={{0,8},{8,16},{16,24},{1,9},{9,17},{17,25},{2,10},{10,18},{18,26},{... | collective-permute-start | bytes 12296 | tf_op jit(solution)/shard_map/ppermute | solution.py:27
  419.8 4.2 copy-start.8
  429.3 81.3 %copy-start.9 = (f32[1024]{0:T(1024)S(1)}, f32[1024]{0:T(1024)}, u32[]{:S(2)}) copy-start(f32[1024]{0:T(1024)} %param.29) | copy-start | bytes 12292
  510.6 125.4 %copy-start.11 = (f32[512]{0:T(512)S(1)}, f32[512]{0:T(512)}, u32[]{:S(2)}) copy-start(f32[512]{0:T(512)} %param.31) | copy-start | bytes 6148
Sparse Core Ops, SparseCore 0:
  8.9 10.2 all-gather.29
  21.9 75.0 all-gather.13
  99.8 74.1 all-gather.15
  176.6 74.1 all-gather.17
  253.5 59.1 all-gather.25
  315.3 59.1 all-gather.23
  376.1 43.6 all-gather.31
  422.5 87.7 all-gather.19
  513.1 59.2 all-gather.21
  574.9 61.0 all-gather.27
  641.6 8.7 reduce-scatter.1
where the time goes:
time: 659 us; the launch traced here: 657 us
  waiting for transfers between devices  574 us (87%)
  matrix products  36.6 us (6%)
  blocking collectives  14.5 us (2%)
  between operations  13.6 us (2%)
  other arithmetic  12.1 us (2%)
    all_gather x1, waiting for transfers between devices, shards(): lax.all_gather(recurrence_output_weight, ('sp', 'fs'), axis=1, tiled=True)  79 us
    all_gather x1, waiting for transfers between devices, shards(): lax.all_gather(query_weight, ('sp', 'fs'), axis=0, tiled=True)  77.9 us
    all_gather x1, waiting for transfers between devices, shards(): lax.all_gather(forget_weight, ('sp', 'fs'), axis=0, tiled=True)  73.2 us
    all_gather x1, waiting for transfers between devices, shards(): lax.all_gather(value_weight, ('sp', 'fs'), axis=0, tiled=True)  72.3 us
    all_gather x1, waiting for transfers between devices, shards(): lax.all_gather(convolution_output_weight, ('sp', 'fs'), axis=1, tiled=True)  63.6 us
    all_gather x1, waiting for transfers between devices, shards(): lax.all_gather(convolution_multiplier_weight, ('sp', 'fs'), axis=0, tiled...  59.2 us
    all_gather x1, waiting for transfers between devices, shards(): lax.all_gather(convolution_gate_weight, ('sp', 'fs'), axis=0, tiled=True)  58.1 us
    all_gather x1, waiting for transfers between devices, shards(): lax.all_gather(convolution_input_weight, ('sp', 'fs'), axis=0, tiled=True)  45.5 us
  transfers between devices with their start and end apart: 12, of which 11 were waited for; matrix products, arithmetic and copies ran while one was open for 7% of the time, Pallas kernels for 0%

commit v1 on v0

--- a/solution.py
+++ b/solution.py
@@ -1,6 +1,10 @@
+import functools
+
 import jax
 import jax.numpy as jnp
 from jax import lax
+from jax.experimental import pallas as pl
+from jax.experimental.pallas import tpu as pltpu
 from jax.sharding import PartitionSpec as P
 
 DK = 128
@@ -184,6 +188,355 @@
     return mixed[None]
 
 
+MESH = pl.DeviceIdType.MESH
+F32 = jnp.float32
+BF16 = jnp.bfloat16
+CONTRACT_LAST = (((1,), (1,)), ((), ()))
+CONTRACT_FIRST = (((0,), (0,)), ((), ()))
+
+
+def layer_kernel(
+    n_sp, n_fs, tok, wq, wf, wv, cg, cm, ci, ro, co, headroom, rate, init, gain, taps, bias,
+    out, tokens, win, wout, rates, state, ext, sib_send, sib_recv, mine, z_send, z_recv,
+    loc_sem, send_sem, win_z, wout_z, win_f, wout_f, tok_z, tok_t, rate_z, sib_sem, zr_sem,
+    rs_send,
+):
+    sp, fs, tp = lax.axis_index("sp"), lax.axis_index("fs"), lax.axis_index("tp")
+    other = 1 - tp
+    rows = wq.shape[0]
+    rec = wq.shape[1] // n_sp
+    con = cg.shape[1] // n_sp
+    span = tok.shape[0]
+    heads = rec // DK
+    wide = tok.shape[1]
+
+    def peer(**where):
+        return {"sp": where.get("sp", sp), "fs": where.get("fs", fs), "tp": where.get("tp", tp)}
+
+    def z_at(d):
+        return lax.rem(sp + d, n_sp)
+
+    def f_at(e):
+        return lax.rem(fs + e, n_fs)
+
+    parts = []
+    at = 0
+    for ref, width in ((wq, rec), (wf, rec), (wv, rec), (cg, con), (cm, con), (ci, con)):
+        parts.append((ref, at, width))
+        at += width
+
+    def in_slot(s, f):
+        return win.at[pl.ds(pl.multiple_of((s * n_fs + f) * rows, rows), rows)]
+
+    def in_piece(s, f, at, width):
+        first = pl.multiple_of((s * n_fs + f) * rows, rows)
+        return win.at[pl.ds(first, rows), pl.ds(at, width)]
+
+    def out_slot(s, f):
+        lanes = ro.shape[1]
+        return wout.at[:, pl.ds(pl.multiple_of((s * n_fs + f) * lanes, lanes), lanes)]
+
+    def out_piece(s, f, at, width):
+        lanes = ro.shape[1]
+        first = pl.multiple_of((s * n_fs + f) * lanes, lanes)
+        return wout.at[pl.ds(at, width), pl.ds(first, lanes)]
+
+    def weight_sources(s):
+        ins = [
+            (ref.at[:, pl.ds(pl.multiple_of(s * width, width), width)], at, width)
+            for ref, at, width in parts
+        ]
+        outs = [
+            (ro.at[pl.ds(pl.multiple_of(s * rec, rec), rec)], 0, rec),
+            (co.at[pl.ds(pl.multiple_of(s * con, con), con)], rec, con),
+        ]
+        return ins, outs
+
+    local = []
+    ins, outs = weight_sources(sp)
+    for ref, at, width in ins:
+        local.append((ref, in_piece(sp, fs, at, width)))
+    for ref, at, width in outs:
+        local.append((ref, out_piece(sp, fs, at, width)))
+    local.append((tok, tokens.at[sp * 2 + tp]))
+    local.append((rate.at[sp], rates.at[sp]))
+    local = [pltpu.make_async_copy(*pair, loc_sem.at[i]) for i, pair in enumerate(local)]
+    for copy in local:
+        copy.start()
+
+    barrier = pltpu.get_barrier_semaphore()
+    for d in range(1, n_sp):
+        pl.semaphore_signal(barrier, inc=1, device_id=peer(sp=z_at(d)), device_id_type=MESH)
+    for e in range(1, n_fs):
+        pl.semaphore_signal(barrier, inc=1, device_id=peer(fs=f_at(e)), device_id_type=MESH)
+    pl.semaphore_signal(barrier, inc=1, device_id=peer(tp=other), device_id_type=MESH)
+    pl.semaphore_wait(barrier, n_sp + n_fs - 1)
+
+    sent = []
+
+    def remote(src, dst, recv, to, start=True):
+        copy = pltpu.make_async_remote_copy(
+            src_ref=src, dst_ref=dst, send_sem=send_sem.at[len(sent) if start else 0], recv_sem=recv, device_id=to,
+            device_id_type=MESH,
+        )
+        if start:
+            copy.start()
+            sent.append(copy)
+        return copy
+
+    near = sorted(range(1, n_sp), key=lambda d: min(d, n_sp - d))
+    for d in near:
+        to = peer(sp=z_at(d))
+        ins, outs = weight_sources(z_at(d))
+        for i, (ref, at, width) in enumerate(ins):
+            remote(ref, in_piece(sp, fs, at, width), win_z.at[d, i], to)
+        for i, (ref, at, width) in enumerate(outs):
+            remote(ref, out_piece(sp, fs, at, width), wout_z.at[d, i], to)
+        remote(tok, tokens.at[sp * 2 + tp], tok_z.at[d], to)
+        remote(rate.at[z_at(d)], rates.at[sp], rate_z.at[d], to)
+    remote(tok, tokens.at[sp * 2 + tp], tok_t.at[0], peer(tp=other))
+
+    for copy in local:
+        copy.wait()
+
+    def spread(d):
+        s = z_at(n_sp - d)
+        for e in range(1, n_fs):
+            remote(in_slot(s, fs), in_slot(s, fs), win_f.at[e, d], peer(fs=f_at(e)))
+        for e in range(1, n_fs):
+            remote(out_slot(s, fs), out_slot(s, fs), wout_f.at[e, d], peer(fs=f_at(e)))
+
+    spread(0)
+    for d in near:
+        s = z_at(n_sp - d)
+        me = peer(tp=other)
+        for i, (ref, at, width) in enumerate(parts):
+            piece = in_piece(s, fs, at, width)
+            remote(piece, piece, win_z.at[d, i], me, start=False).wait_recv()
+        for i, (at, width) in enumerate(((0, rec), (rec, con))):
+            piece = out_piece(s, fs, at, width)
+            remote(piece, piece, wout_z.at[d, i], me, start=False).wait_recv()
+        spread(d)
+        piece = tokens.at[s * 2 + tp]
+        remote(piece, piece, tok_z.at[d], me, start=False).wait_recv()
+        remote(piece, piece, tok_t.at[d], me)
+        remote(rates.at[s], rates.at[s], rate_z.at[d], me, start=False).wait_recv()
+    for d in range(n_sp):
+        s = z_at((n_sp - d) % n_sp)
+        piece = tokens.at[s * 2 + other]
+        remote(piece, piece, tok_t.at[d], peer(tp=other), start=False).wait_recv()
+    for d in range(n_sp):
+        s = z_at((n_sp - d) % n_sp)
+        for e in range(1, n_fs):
+            f = f_at(n_fs - e)
+            remote(in_slot(s, f), in_slot(s, f), win_f.at[e, d], peer(tp=other), start=False).wait_recv()
+            remote(out_slot(s, f), out_slot(s, f), wout_f.at[e, d], peer(tp=other), start=False).wait_recv()
+    for copy in sent:
+        copy.wait_send()
+
+    for h in range(heads):
+        state[h] = init[sp * heads + h].T
+    ext[0:8] = jnp.zeros((8, con), F32)
+    lane_rec = pl.ds(pl.multiple_of(sp * rec, rec), rec)
+    lane_con = pl.ds(pl.multiple_of(sp * con, con), con)
+    row_id = lax.broadcasted_iota(jnp.int32, (span, span), 0)
+    col_id = lax.broadcasted_iota(jnp.int32, (span, span), 1)
+    causal = row_id >= col_id
+    lower = causal.astype(F32)
+    upper = (row_id <= col_id).astype(F32)
+    length = 2 * span
+
+    def sib_copy(s):
+        return pltpu.make_async_remote_copy(
+            src_ref=sib_send.at[s], dst_ref=sib_recv.at[s], send_sem=rs_send.at[0, s],
+            recv_sem=sib_sem.at[s], device_id=peer(tp=other), device_id_type=MESH,
+        )
+
+    def z_copy(s):
+        d = lax.rem(s - sp + n_sp, n_sp)
+        return pltpu.make_async_remote_copy(
+            src_ref=z_send.at[s], dst_ref=z_recv.at[d], send_sem=rs_send.at[1, d],
+            recv_sem=zr_sem.at[d], device_id=peer(sp=s), device_id_type=MESH,
+        )
+
+    def pass_on(s):
+        sib_copy(s).wait_recv()
+        total = mine[s] + sib_recv[s].astype(F32)
+
+        @pl.when(s != sp)
+        def _():
+            z_send[s] = total.astype(BF16)
+            z_copy(s).start()
+
+        @pl.when(s == sp)
+        def _():
+            z_recv[0] = total.astype(BF16)
+
+    def step(s, carry):
+        block = jnp.concatenate([tokens[2 * s], tokens[2 * s + 1]], axis=0)
+
+        def project(at, width):
+            return jnp.dot(
+                block, win[:, pl.ds(at, width)], preferred_element_type=F32
+            ).astype(BF16)
+
+        query = project(0, rec).astype(F32) * DK ** (-0.5)
+        forget = project(rec, rec).astype(F32)
+        value = project(2 * rec, rec)
+        base = 3 * rec
+        conv_gate = project(base, con).astype(F32)
+        prod = project(base + con, con).astype(F32) * project(base + 2 * con, con).astype(F32)
+        key_gate = headroom[:, lane_rec] * jax.nn.sigmoid(-forget)
+        log_forget = jnp.log1p(-key_gate)
+        gains = gain[:, lane_rec]
+        halves = []
+        for c in range(2):
+            part = slice(c * span, (c + 1) * span)
+            cum = jnp.dot(lower, log_forget[part], precision=lax.Precision.HIGHEST)
+            extra = jnp.dot(rates[s][:, part], upper, precision=lax.Precision.HIGHEST)
+            extra_t = extra.T
+            grow = jnp.exp(cum)
+            query_grow = query[part] * grow
+            key_grow = (key_gate[part] / grow).astype(BF16)
+            last = cum[span - 1 :, :]
+            key_last = key_gate[part] * jnp.exp(last - cum)
+            last_decay = jnp.exp(last)
+            pieces = []
+            for h in range(heads):
+                lanes = slice(h * DK, (h + 1) * DK)
+                row = extra[h : h + 1]
+                column = extra_t[:, h : h + 1]
+                end = row[:, span - 1 :]
+                scores = lax.dot_general(
+                    query_grow[:, lanes].astype(BF16), key_grow[:, lanes], CONTRACT_LAST,
+                    preferred_element_type=F32,
+                )
+                decay = jnp.exp(jnp.where(causal, column - row, 0.0))
+                scores = jnp.where(causal, scores * decay, 0.0).astype(BF16)
+                values = value[part, lanes]
+                before = state[h]
+                raw = jnp.dot(scores, values, preferred_element_type=F32)
+                raw = raw + lax.dot_general(
+                    (query_grow[:, lanes] * jnp.exp(column)).astype(BF16), before.astype(BF16),
+                    CONTRACT_LAST, preferred_element_type=F32,
+                )
+                keys = (key_last[:, lanes] * jnp.exp(end - column)).astype(BF16)
+                state[h] = before * (last_decay[:, lanes] * jnp.exp(end)) + lax.dot_general(
+                    values, keys, CONTRACT_FIRST, preferred_element_type=F32
+                )
+                square = jnp.mean(raw * raw, axis=-1, keepdims=True)
+                pieces.append((raw * lax.rsqrt(square + 1e-06) * gains[:, lanes]).astype(BF16))
+            halves.append(jnp.concatenate(pieces, axis=1))
+        ext[8:] = prod
+        conv = jnp.broadcast_to(bias[:, lane_con], prod.shape)
+        for j in range(KW):
+            conv = conv + taps[j : j + 1, lane_con] * ext[pl.ds(8 - (KW - 1) + j, length)]
+        ext[0:8] = ext[length:]
+        conv_out = (conv_gate * conv).astype(BF16)
+        both = jnp.concatenate([jnp.concatenate(halves, axis=0), conv_out], axis=1)
+        chunk = min(512, wide)
+        for n in range(0, wide, chunk):
+            partial = jnp.dot(both, wout[:, n : n + chunk], preferred_element_type=F32)
+            first = partial[:span]
+            second = partial[span:]
+            mine[s, :, n : n + chunk] = jnp.where(tp == 0, first, second)
+            sib_send[s, :, n : n + chunk] = jnp.where(tp == 0, second, first).astype(BF16)
+        sib_copy(s).start()
+
+        @pl.when(s > 0)
+        def _():
+            pass_on(s - 1)
+
+        return carry
+
+    lax.fori_loop(0, n_sp, step, 0)
+    pass_on(n_sp - 1)
+    for d in range(1, n_sp):
+        pltpu.make_async_remote_copy(
+            src_ref=z_recv.at[d], dst_ref=z_recv.at[d], send_sem=rs_send.at[1, d],
+            recv_sem=zr_sem.at[d], device_id=peer(tp=other), device_id_type=MESH,
+        ).wait_recv()
+    total = z_recv[0].astype(F32)
+    for d in range(1, n_sp):
+        total = total + z_recv[d].astype(F32)
+    out[...] = total.astype(BF16)
+    for s in range(n_sp):
+        sib_copy(s).wait_send()
+    for d in range(1, n_sp):
+        pltpu.make_async_remote_copy(
+            src_ref=z_send.at[z_at(d)], dst_ref=z_recv.at[d], send_sem=rs_send.at[1, d],
+            recv_sem=zr_sem.at[d], device_id=peer(sp=z_at(d)), device_id_type=MESH,
+        ).wait_send()
+
+
+def sequence_shards(n_sp, n_fs, *arrays):
+    (tok, wq, wf, wv, cg, cm, ci, headroom, rate, init, gain, taps, bias, ro, co) = arrays
+    span, wide = tok.shape[1:]
+    rec, con = wq.shape[1] // n_sp, cg.shape[1] // n_sp
+    heads = rec // DK
+    by_place = rate[0].reshape(n_sp, heads, rate.shape[2])
+    by_place = jnp.pad(by_place, ((0, 0), (0, 8 - heads), (0, 0)))
+    hbm = pl.BlockSpec(memory_space=pl.ANY)
+    vmem = pl.BlockSpec(memory_space=pltpu.VMEM)
+    dma = pltpu.SemaphoreType.DMA
+    mixed = pl.pallas_call(
+        functools.partial(layer_kernel, n_sp, n_fs),
+        out_shape=jax.ShapeDtypeStruct((span, wide), BF16),
+        in_specs=[hbm] * 9 + [vmem, hbm] + [vmem] * 4,
+        out_specs=vmem,
+        scratch_shapes=[
+            pltpu.VMEM((2 * n_sp, span, wide), BF16),
+            pltpu.VMEM((wide, 3 * (rec + con)), BF16),
+            pltpu.VMEM((rec + con, wide), BF16),
+            pltpu.VMEM((n_sp, 8, rate.shape[2]), F32),
+            pltpu.VMEM((heads, DK, DK), F32),
+            pltpu.VMEM((8 + 2 * span, con), F32),
+            pltpu.VMEM((n_sp, span, wide), BF16),
+            pltpu.VMEM((n_sp, span, wide), BF16),
+            pltpu.VMEM((n_sp, span, wide), F32),
+            pltpu.VMEM((n_sp, span, wide), BF16),
+            pltpu.VMEM((n_sp, span, wide), BF16),
+            dma((10,)),
+            dma(((n_sp - 1) * 10 + n_sp * (1 + 2 * (n_fs - 1)),)),
+            dma((n_sp, 6)),
+            dma((n_sp, 2)),
+            dma((n_fs, n_sp)),
+            dma((n_fs, n_sp)),
+            dma((n_sp,)),
+            dma((n_sp,)),
+            dma((n_sp,)),
+            dma((n_sp,)),
+            dma((n_sp,)),
+            dma((2, n_sp)),
+        ],
+        compiler_params=pltpu.CompilerParams(
+            collective_id=0, has_side_effects=True, vmem_limit_bytes=60 * 2**20
+        ),
+    )(
+        tok[0], wq, wf, wv, cg, cm, ci, ro, co, headroom[None], by_place, init[0], gain[None],
+        taps, bias[None],
+    )
+    return mixed[None]
+
+
+def choose_plan(sizes, *arrays):
+    n_sp, n_fs = sizes["sp"], sizes["fs"]
+    rows, rec = arrays[1].shape
+    con = arrays[4].shape[1]
+    span = arrays[0].shape[1]
+    even = (
+        sizes["tp"] == 2
+        and arrays[0].shape[0] == 1
+        and rec % (n_sp * DK) == 0
+        and rec // (n_sp * DK) <= 8
+        and con % (n_sp * 128) == 0
+        and rows % 128 == 0
+        and span == DK
+        and arrays[13].shape[1] % 128 == 0
+    )
+    return sequence_shards(n_sp, n_fs, *arrays) if even else shards(*arrays)
+
+
 def solution(mesh):
     in_specs = (
         P("fs", ("sp", "tp"), None),
@@ -203,4 +556,5 @@
         P("tp", ("sp", "fs")),
     )
     out_specs = P("fs", ("sp", "tp"), None)
-    return jax.shard_map(shards, mesh=mesh, in_specs=in_specs, out_specs=out_specs, check_vma=False)
+    body = functools.partial(choose_plan, dict(mesh.shape))
+    return jax.shard_map(body, mesh=mesh, in_specs=in_specs, out_specs=out_specs, check_vma=False)

time: 659 us -> 150 us (0.23)
  waiting for transfers between devices: 574 us -> 0 us
  Pallas kernels: 0 us -> 147 us
  matrix products: 36.6 us -> 0 us
  blocking collectives: 14.5 us -> 0 us
  between operations: 13.6 us -> 0.01 us
  other arithmetic: 12.1 us -> 0 us
    all_gather x10 -> x0, waiting for transfers between devices: 559 us -> none  [the longest x1 79 us: shards(): lax.all_gather(recurrence_output_weight, ('sp', 'fs'), axis=1, tiled=True)]
    pallas_call x0 -> x1, Pallas kernels: none -> 147 us  [sequence_shards(): pl.pallas_call(functools.partial(layer_kernel, n_sp, n_fs), out_shape=jax...]
    dot_general x11 -> x0, matrix products: 36.6 us -> none  [the longest x5 16.8 us: shards(): jnp.dot(block_rows, weight, preferred_element_type=jnp.float32)]
    all_gather x1 -> x0, blocking collectives: 14.5 us -> none  [carried_in(): gathered = jax.tree.map(lambda a: lax.all_gather(a, axis), part)]
    reduce_scatter x1 -> x0, waiting for transfers between devices: 8.94 us -> none  [shards(): lax.psum_scatter((jnp.dot(rec_out, out_rec, preferred_element_type=jnp.fl...]
  transfers between devices with their start and end apart: 12 -> 0, of which waited for: 11 -> 0; matrix products, arithmetic and copies ran while one was open for 7% -> 0% of each run, Pallas kernels for 0% -> 0%
where the time goes in v1:
time: 150 us
  Pallas kernels  147 us (98%)
  local copies, waits for them, and re-layouts  3.21 us (2%)
    pallas_call x1, Pallas kernels, sequence_shards(): pl.pallas_call(functools.partial(layer_kernel, n_sp, n_fs), out_shape=jax...  147 us

profile of v1, /device:TPU:28, one launch (start us, length us, event | category | flops | bytes accessed | tf_op | source)
XLA Modules:
  0.0 150.1 jit_solution(13416257417172974741)
XLA Ops:
  0.0 0.0 copy-start
  0.0 0.7 copy-done
  0.7 0.6 pad.4.rate
  1.3 146.9 %shard_map.145 = bf16[128,2048]{1,0:T(8,128)(2,1)} custom-call(bf16[128,2048]{1,0:T(8,128)(2,1)} %bitcast.7, bf16[128,1024]{1,0:T(8,128)(2,1)} %wq.1, bf16[128,1024]{1,0:T(8,128)(2,1)} %wf.1, bf16[128,1024]{1,0:T(8,128)(2,1)} %wv.1, bf16[128,512]{1,0:T(8,128)(2,1)} %cg.1, bf16[128,512]{1,0:T(8,128)(2,1)} %cm.1, bf16[128,512]{1,0:T(8,128)(2,1)} %ci.1, ...), custom_call_target="tpu_custom_call" | custom-call | tf_op jit(solution)/shard_map/pallas_call | solution.py:482
  148.2 1.9 %copy.17 = bf16[1,128,2048]{2,1,0:T(8,128)(2,1)} copy(bf16[1,128,2048]{2,1,0:T(8,128)(2,1)} %bitcast.6) | data formatting | bytes 1048576
  (1 shorter events, 0.0 us)
Async XLA Ops:
  0.0 0.7 copy-start
